TPU v7x, 256 devices: a whole 4x4x8 slice. The times are simulated.
256 devices in a mesh: sp: 32 (over z, x), tp: 8 (over y, core).
Axes of the slice: x: 4, y: 4, z: 8, core: 2. Of those that a mesh axis runs over, the one named last changes fastest.
Arguments:
- out_grad: bfloat16 [4096, 2048], P('sp', 'tp'), may hold values from -6 to 6
- moe_input: bfloat16 [4096, 2048], P('sp', 'tp'), may hold values from -6 to 6
- route_weight: float32 [4096, 2], P('sp'), may hold values from 0.2 to 1
- route_ids: int32 [4096, 2], P('sp'), may hold values from 0 to 31, all different within a row; in each aligned block of 128 rows (0 to 127, 128 to 255, ...) at most 16 rows name the same one
- gate_proj: bfloat16 [32, 2048, 2816], P('sp', None, 'tp'), may hold values from -0.125 to 0.125
- up_proj: bfloat16 [32, 2048, 2816], P('sp', None, 'tp'), may hold values from -0.125 to 0.125
- down_proj: bfloat16 [32, 2816, 2048], P('sp', 'tp'), may hold values from -0.109375 to 0.109375
- out_proj: bfloat16 [2048, 2048], P(None, 'tp'), may hold values from -0.125 to 0.125
- conv_out: bfloat16 [4096, 2048], P('sp', 'tp'), may hold values from -6 to 6
- gate_b: bfloat16 [4096, 2048], P('sp', 'tp'), may hold values from -6 to 6
- gate_c: bfloat16 [4096, 2048], P('sp', 'tp'), may hold values from -6 to 6
- value_v: bfloat16 [4096, 2048], P('sp', 'tp'), may hold values from -6 to 6
- conv_taps: float32 [3, 2048], P(None, 'tp'), may hold values from -3 to 3
Outputs:
- grad_gate: bfloat16 [32, 2048, 2816], P('sp', None, 'tp')
- grad_up: bfloat16 [32, 2048, 2816], P('sp', None, 'tp')
- grad_down: bfloat16 [32, 2816, 2048], P('sp', 'tp')
- grad_out: float32 [2048, 2048], P('sp', 'tp')
- grad_b: bfloat16 [4096, 2048], P('sp', 'tp')
- grad_c: bfloat16 [4096, 2048], P('sp', 'tp')
- grad_v: bfloat16 [4096, 2048], P('sp', 'tp')
Inputs may be any that keep to these rules, and one draw needn't show every extreme that they name: `route_ids`: each row names two different experts; within the 128 rows of one index of sp no expert is named by more than 16 rows, a bound that some block reaches.
All inputs are finite; a program needn't handle non-finite values.
Results may differ from a plain program's by a relative error of at most 0.019.
Values may be sent and summed in bfloat16 or wider, within the bound.
A program may use at most 64 MiB of HBM per device.

v0:
```python
import functools

import jax
import jax.numpy as jnp
from jax import lax
from jax.experimental import pallas as pl
from jax.experimental.pallas import tpu as pltpu
from jax.sharding import PartitionSpec as P

MESH = pl.DeviceIdType.MESH


def place(n, q):
    s, t = lax.axis_index("sp"), lax.axis_index("tp")
    sibling = t + 1 - 2 * lax.rem(t, 2)
    return s, t, sibling


def greet(n, q):
    s, t, sibling = place(n, q)
    barrier = pltpu.get_barrier_semaphore()
    for i in range(1, n):
        pl.semaphore_signal(
            barrier, inc=1, device_id=(lax.rem(s + i, n), t), device_id_type=MESH
        )
    for d in range(1, q // 2):
        pl.semaphore_signal(
            barrier, inc=1, device_id=(s, lax.rem(t + 2 * d, q)), device_id_type=MESH
        )
    pl.semaphore_signal(barrier, inc=1, device_id=(s, sibling), device_id_type=MESH)
    return barrier, n - 1 + q // 2


def remote(src, dst, send_sem, recv_sem, device):
    return pltpu.make_async_remote_copy(
        src_ref=src,
        dst_ref=dst,
        send_sem=send_sem,
        recv_sem=recv_sem,
        device_id=device,
        device_id_type=MESH,
    )


def dispatch_kernel(
    n, q, ids_ref, w_ref, x_ref, g_ref, xo_ref, do_ref, p_ref,
    p01, send, buf, out_sem, s1, r1, sy, ry, ss, rs,
):
    s, t, sibling = place(n, q)
    ny = q // 2
    tok, cols = x_ref.shape
    total = send.shape[1]
    cap = total // n
    barrier, greeted = greet(n, q)

    ids0, ids1 = ids_ref[0:1, :], ids_ref[1:2, :]
    experts = lax.broadcasted_iota(jnp.int32, (n, tok), 0)
    named = jnp.logical_or(ids0 == experts, ids1 == experts)
    named_f = jnp.where(named, 1.0, 0.0)
    earlier = jnp.where(
        lax.broadcasted_iota(jnp.int32, (tok, tok), 0)
        < lax.broadcasted_iota(jnp.int32, (tok, tok), 1),
        1.0,
        0.0,
    )
    before = jnp.dot(
        named_f.astype(jnp.bfloat16),
        earlier.astype(jnp.bfloat16),
        preferred_element_type=jnp.float32,
    ).astype(jnp.int32)
    slots = lax.broadcasted_iota(jnp.int32, (cap, tok), 0)
    for e in range(n):
        here = before[e : e + 1, :] == slots
        c0 = jnp.where(jnp.logical_and(here, ids0 == e), 1.0, 0.0)
        c1 = jnp.where(jnp.logical_and(here, ids1 == e), 1.0, 0.0)
        rows = slice(e * cap, (e + 1) * cap)
        p01[rows, 0:tok] = c0.astype(jnp.bfloat16)
        p01[rows, tok : 2 * tok] = c1.astype(jnp.bfloat16)
        p_ref[rows, :] = (c0 + c1).astype(jnp.bfloat16)
    grad = g_ref[...].astype(jnp.float32)
    weighted = jnp.concatenate(
        [
            (w_ref[:, 0:1] * grad).astype(jnp.bfloat16),
            (w_ref[:, 1:2] * grad).astype(jnp.bfloat16),
        ],
        axis=0,
    )
    send[0] = jnp.dot(p_ref[...], x_ref[...], preferred_element_type=jnp.float32).astype(
        jnp.bfloat16
    )
    send[1] = jnp.dot(p01[...], weighted, preferred_element_type=jnp.float32).astype(jnp.bfloat16)

    def at_rows(j):
        return pl.ds(pl.multiple_of(j * cap, cap), cap)

    def block(j, tt):
        return buf.at[:, at_rows(j), pl.ds(pl.multiple_of(tt * cols, cols), cols)]

    def first(i):
        e = lax.rem(s + i, n)
        return remote(send.at[:, at_rows(e)], block(s, t), s1.at[i], r1.at[i], (e, t))

    def across(i, d):
        j = lax.rem(s - i + n, n)
        b = block(j, t)
        return remote(b, b, sy.at[i, d - 1], ry.at[i, d - 1], (s, lax.rem(t + 2 * d, q)))

    def beside(i, d):
        j = lax.rem(s - i + n, n)
        b = block(j, lax.rem(t - 2 * d + q, q))
        return remote(b, b, ss.at[i, d], rs.at[i, d], (s, sibling))

    pl.semaphore_wait(barrier, greeted)
    own = pltpu.make_async_copy(send.at[:, at_rows(s)], block(s, t), s1.at[0])
    own.start()
    for i in range(1, n):
        first(i).start()

    def forward(i):
        for d in range(1, ny):
            across(i, d).wait_recv()
            beside(i, d).start()

    outs = []

    def drain(i):
        j = lax.rem(s - i + n, n)
        for d in range(ny):
            beside(i, d).wait_recv()
        for a, ref in enumerate((xo_ref, do_ref)):
            copy = pltpu.make_async_copy(
                buf.at[a, at_rows(j)], ref.at[at_rows(j)], out_sem.at[i, a]
            )
            copy.start()
            outs.append(copy)

    for i in range(n):
        if i == 0:
            own.wait()
        else:
            first(i).wait_recv()
        for d in range(1, ny):
            across(i, d).start()
        beside(i, 0).start()
        if i >= 1:
            forward(i - 1)
        if i >= 2:
            drain(i - 2)
    forward(n - 1)
    for i in range(max(n - 2, 0), n):
        drain(i)
    for i in range(n):
        if i:
            first(i).wait_send()
        for d in range(1, ny):
            across(i, d).wait_send()
        for d in range(ny):
            beside(i, d).wait_send()
    for copy in outs:
        copy.wait()


def dispatch(n, q, ids_t, weight, x, g):
    tok, cols = x.shape
    total = 4 * tok
    ny = q // 2
    vmem = pl.BlockSpec(memory_space=pltpu.VMEM)
    hbm = pl.BlockSpec(memory_space=pl.ANY)
    dma = pltpu.SemaphoreType.DMA
    rows = jax.ShapeDtypeStruct((total, q * cols), jnp.bfloat16)
    return pl.pallas_call(
        functools.partial(dispatch_kernel, n, q),
        out_shape=(rows, rows, jax.ShapeDtypeStruct((total, tok), jnp.bfloat16)),
        in_specs=[vmem] * 4,
        out_specs=(hbm, hbm, vmem),
        scratch_shapes=[
            pltpu.VMEM((total, 2 * tok), jnp.bfloat16),
            pltpu.VMEM((2, total, cols), jnp.bfloat16),
            pltpu.VMEM((2, total, q * cols), jnp.bfloat16),
            dma((n, 2)),
            dma((n,)),
            dma((n,)),
            dma((n, max(ny - 1, 1))),
            dma((n, max(ny - 1, 1))),
            dma((n, ny)),
            dma((n, ny)),
        ],
        compiler_params=pltpu.CompilerParams(collective_id=0, has_side_effects=True),
        name="dispatch",
    )(ids_t, weight, x, g)


def combine_kernel(
    n, q, part_ref, p_ref, g_ref, b_ref, co_ref, c_ref, v_ref, taps_ref, w_hbm,
    x_hbm, dy_hbm, hid_hbm, dg_hbm, du_hbm,
    gout_ref, gb_ref, gc_ref, gv_ref, ggate_hbm, gup_hbm, gdown_hbm,
    rsib, pair, ryb, fin, ret, full_h, h_t, all_t, all_m, w_ref, edge, got, padded,
    x_v, dy_v, hid_v, dg_v, du_v, ggate_v, gup_v, gdown_v, in_sem, o_sem, w_sem,
    ss, rs, sy, ry, s3, r3, sm, rm, sp, rp, shy, rhy, shs, rhs, sa, ra, se, re,
):
    s, t, sibling = place(n, q)
    partner = s + 1 - 2 * lax.rem(s, 2)
    ny = q // 2
    tok, cols = g_ref.shape
    total, width = part_ref.shape
    cap = total // n
    share = width // n
    barrier, greeted = greet(n, q)
    w_copy = pltpu.make_async_copy(w_hbm, w_ref, w_sem)
    loads = [
        pltpu.make_async_copy(source, target, in_sem.at[k])
        for k, (source, target) in enumerate(
            zip((hid_hbm, dy_hbm, x_hbm, dg_hbm, du_hbm), (hid_v, dy_v, x_v, dg_v, du_v))
        )
    ]
    w_copy.start()
    for load in loads:
        load.start()
    all_m[s] = (b_ref[...].astype(jnp.float32) * co_ref[...].astype(jnp.float32)).astype(
        jnp.bfloat16
    )

    def at_rows(j):
        return pl.ds(pl.multiple_of(j * cap, cap), cap)

    def at_cols(tt):
        return pl.ds(pl.multiple_of(tt * cols, cols), cols)

    def beside(i, d):
        j = lax.rem(s + i, n)
        theirs = lax.rem(sibling + 2 * d, q)
        return remote(
            part_ref.at[at_rows(j), at_cols(theirs)],
            rsib.at[d, at_rows(j)],
            ss.at[i, d],
            rs.at[i, d],
            (s, sibling),
        )

    def across(i, d):
        j = lax.rem(s + i, n)
        return remote(
            pair.at[d - 1, at_rows(j)],
            ryb.at[d - 1, at_rows(j)],
            sy.at[i, d - 1],
            ry.at[i, d - 1],
            (s, lax.rem(t + 2 * d, q)),
        )

    def back(i):
        j = lax.rem(s + i, n)
        return remote(fin.at[at_rows(j)], ret.at[at_rows(s)], s3.at[i], r3.at[i], (j, t))

    def mixed_far(i):
        return remote(
            all_m.at[s], all_m.at[s], sm.at[i // 2], rm.at[i // 2], (lax.rem(s + i, n), t)
        )

    def mixed_near(i):
        b = all_m.at[lax.rem(s - i + n, n)]
        return remote(b, b, sp.at[i // 2], rp.at[i // 2], (partner, t))

    def h_across(d):
        b = full_h.at[:, at_cols(t)]
        return remote(b, b, shy.at[d - 1], rhy.at[d - 1], (s, lax.rem(t + 2 * d, q)))

    def h_beside(d):
        b = full_h.at[:, at_cols(lax.rem(t - 2 * d + q, q))]
        return remote(b, b, shs.at[d], rhs.at[d], (s, sibling))

    def h_share(j):
        return pl.ds(pl.multiple_of(j * share, share), share)

    def h_far(i):
        j = lax.rem(s + i, n)
        return remote(h_t.at[h_share(j)], all_t.at[s], sa.at[i], ra.at[i], (j, t))

    def halo(k):
        there = lax.rem(s + 1, n) if k == 0 else lax.rem(s - 1 + n, n)
        return remote(edge.at[k], got.at[k], se.at[k], re.at[k], (there, t))

    plain = (((1,), (0,)), ((), ()))
    stores = [
        pltpu.make_async_copy(source, target, o_sem.at[k])
        for k, (source, target) in enumerate(
            zip((gdown_v, ggate_v, gup_v), (gdown_hbm, ggate_hbm, gup_hbm))
        )
    ]

    def grad_step(left, right, target):
        def step(k, _):
            here = at_cols(k)
            target[:, here] = lax.dot_general(
                left[...], right[:, here], plain, preferred_element_type=jnp.float32
            ).astype(jnp.bfloat16)
            return 0

        return step

    def mine(j, d):
        value = part_ref[at_rows(j), at_cols(lax.rem(t + 2 * d, q))].astype(jnp.float32)
        return value + rsib[d, at_rows(j), :].astype(jnp.float32)

    order = [i % n for i in range(1, n + 1)]
    pl.semaphore_wait(barrier, greeted)
    for i in order:
        for d in [*range(1, ny), 0]:
            beside(i, d).start()
    for i in range(2, n, 2):
        mixed_far(i).start()
    mixed_near(0).start()

    def finish(i):
        j = lax.rem(s + i, n)
        beside(i, 0).wait_recv()
        value = mine(j, 0)
        for d in range(1, ny):
            across(i, d).wait_recv()
            value = value + ryb[d - 1, at_rows(j), :].astype(jnp.float32)
        value = value.astype(jnp.bfloat16)
        if i == 0:
            ret[at_rows(s), :] = value
        else:
            fin[at_rows(j), :] = value
            back(i).start()

    for k, i in enumerate(order):
        j = lax.rem(s + i, n)
        for d in range(1, ny):
            beside(i, d).wait_recv()
            pair[d - 1, at_rows(j), :] = mine(j, d).astype(jnp.bfloat16)
            across(i, d).start()
        if k >= 1:
            finish(order[k - 1])
    finish(order[-1])
    for i in range(2, n, 2):
        mixed_far(i).wait_recv()
        mixed_near(i).start()
    for load in loads:
        load.wait()
    lax.fori_loop(0, q, grad_step(hid_v, dy_v, gdown_v), 0)
    stores[0].start()
    for i in range(1, n):
        back(i).wait_recv()
    moe = lax.dot_general(
        p_ref[...], ret[...], (((0,), (0,)), ((), ())), preferred_element_type=jnp.float32
    )
    full_h[:, at_cols(t)] = (g_ref[...].astype(jnp.float32) + moe).astype(jnp.bfloat16)
    for d in range(1, ny):
        h_across(d).start()
    h_beside(0).start()
    w_copy.wait()
    for d in range(1, ny):
        h_across(d).wait_recv()
        h_beside(d).start()
    for d in range(ny):
        h_beside(d).wait_recv()
    for k in range(q):
        here = slice(k * cols, (k + 1) * cols)
        h_t[here, :] = full_h[:, here].astype(jnp.float32).T.astype(jnp.bfloat16)
    for i in range(1, n):
        h_far(i).start()
    all_t[s] = h_t[h_share(s), :]
    grad_z = jnp.dot(full_h[...], w_ref[...], preferred_element_type=jnp.float32)
    dconv = (grad_z * b_ref[...].astype(jnp.float32)).astype(jnp.bfloat16).astype(jnp.float32)
    edge[0] = jnp.broadcast_to(dconv[tok - 1 : tok, :], (8, cols))
    edge[1] = jnp.broadcast_to(dconv[0:1, :], (8, cols))
    halo(0).start()
    halo(1).start()
    gb_ref[...] = (grad_z * co_ref[...].astype(jnp.float32)).astype(jnp.bfloat16)
    padded[8 : 8 + tok, :] = dconv
    halo(0).wait_recv()
    halo(1).wait_recv()
    padded[0:8, :] = jnp.where(s > 0, got[0], 0.0)
    padded[8 + tok : 16 + tok, :] = jnp.where(s < n - 1, got[1], 0.0)
    grad_u = (
        taps_ref[0:1, :] * padded[9 : 9 + tok, :]
        + taps_ref[1:2, :] * padded[8 : 8 + tok, :]
        + taps_ref[2:3, :] * padded[7 : 7 + tok, :]
    )
    gc_ref[...] = (grad_u * v_ref[...].astype(jnp.float32)).astype(jnp.bfloat16)
    gv_ref[...] = (grad_u * c_ref[...].astype(jnp.float32)).astype(jnp.bfloat16)
    lax.fori_loop(0, q, grad_step(dg_v, x_v, ggate_v), 0)
    stores[1].start()
    lax.fori_loop(0, q, grad_step(du_v, x_v, gup_v), 0)
    stores[2].start()
    for i in range(0, n, 2):
        mixed_near(i).wait_recv()
    for i in range(1, n):
        h_far(i).wait_recv()
    total_out = jnp.zeros((share, cols), jnp.float32)
    for k in range(n):
        total_out = total_out + jnp.dot(all_t[k], all_m[k], preferred_element_type=jnp.float32)
    gout_ref[...] = total_out
    for i in range(n):
        if i:
            back(i).wait_send()
            h_far(i).wait_send()
        if i % 2 == 0:
            mixed_near(i).wait_send()
            if i:
                mixed_far(i).wait_send()
        for d in range(1, ny):
            across(i, d).wait_send()
        for d in range(ny):
            beside(i, d).wait_send()
    for d in range(ny):
        if d:
            h_across(d).wait_send()
        h_beside(d).wait_send()
    halo(0).wait_send()
    halo(1).wait_send()
    for store in stores:
        store.wait()


def combine(
    n, q, part, p, g, gate_b, conv_out, gate_c, value_v, taps, out_proj, x, dy, hid, dg, du
):
    total, width = part.shape
    tok, cols = g.shape
    share = width // n
    ny = q // 2
    far = max(ny - 1, 1)
    vmem = pl.BlockSpec(memory_space=pltpu.VMEM)
    dma = pltpu.SemaphoreType.DMA
    half = jnp.bfloat16
    like = jax.ShapeDtypeStruct(g.shape, half)
    hbm = pl.BlockSpec(memory_space=pl.ANY)
    units = hid.shape[0]
    tall = (units, width)
    sems = [(n, ny), (n, far), (n,), (n // 2,), (n // 2,), (far,), (ny,), (n,), (2,)]
    return pl.pallas_call(
        functools.partial(combine_kernel, n, q),
        out_shape=(
            jax.ShapeDtypeStruct((share, cols), jnp.float32),
            like,
            like,
            like,
            jax.ShapeDtypeStruct(tall, half),
            jax.ShapeDtypeStruct(tall, half),
            jax.ShapeDtypeStruct(tall, half),
        ),
        in_specs=[vmem] * 8 + [hbm] * 6,
        out_specs=(vmem,) * 4 + (hbm,) * 3,
        scratch_shapes=[
            pltpu.VMEM((ny, total, cols), half),
            pltpu.VMEM((far, total, cols), half),
            pltpu.VMEM((far, total, cols), half),
            pltpu.VMEM((total, cols), half),
            pltpu.VMEM((total, cols), half),
            pltpu.VMEM((tok, width), half),
            pltpu.VMEM((width, tok), half),
            pltpu.VMEM((n, share, tok), half),
            pltpu.VMEM((n, tok, cols), half),
            pltpu.VMEM(out_proj.shape, half),
            pltpu.VMEM((2, 8, cols), jnp.float32),
            pltpu.VMEM((2, 8, cols), jnp.float32),
            pltpu.VMEM((tok + 16, cols), jnp.float32),
            pltpu.VMEM((total, width), half),
            pltpu.VMEM((total, width), half),
            pltpu.VMEM((units, total), half),
            pltpu.VMEM((units, total), half),
            pltpu.VMEM((units, total), half),
            pltpu.VMEM(tall, half),
            pltpu.VMEM(tall, half),
            pltpu.VMEM(tall, half),
            dma((5,)),
            dma((3,)),
            dma,
        ]
        + [dma(shape) for shape in sems for _ in range(2)],
        compiler_params=pltpu.CompilerParams(collective_id=1, has_side_effects=True, vmem_limit_bytes=30 * 2**20),
        name="combine",
    )(part, p, g, gate_b, conv_out, gate_c, value_v, taps, out_proj, x, dy, hid, dg, du)


def local(
    out_grad,
    moe_input,
    route_weight,
    route_ids,
    gate_proj,
    up_proj,
    down_proj,
    out_proj,
    conv_out,
    gate_b,
    gate_c,
    value_v,
    conv_taps,
):
    n = lax.axis_size("sp")
    q = lax.axis_size("tp")
    xin, dyin, slots = dispatch(n, q, route_ids.T, route_weight, moe_input, out_grad)
    w_gate = gate_proj[0]
    w_up = up_proj[0]
    w_down = down_proj[0]
    gate = jnp.dot(xin, w_gate, preferred_element_type=jnp.float32)
    upval = jnp.dot(xin, w_up, preferred_element_type=jnp.float32)
    sig = jax.nn.sigmoid(gate)
    act = gate * sig
    hidden = (act * upval).astype(jnp.bfloat16)
    dhid = jnp.dot(dyin, w_down.T, preferred_element_type=jnp.float32)
    dgate = (dhid * upval * (sig * (1.0 + gate * (1.0 - sig)))).astype(jnp.bfloat16)
    dup = (dhid * act).astype(jnp.bfloat16)
    partial_value = jnp.dot(dgate, w_gate.T, preferred_element_type=jnp.float32) + jnp.dot(
        dup, w_up.T, preferred_element_type=jnp.float32
    )
    grad_out, grad_b, grad_c, grad_v, grad_gate, grad_up, grad_down = combine(
        n,
        q,
        partial_value.astype(jnp.bfloat16),
        slots,
        out_grad,
        gate_b,
        conv_out,
        gate_c,
        value_v,
        conv_taps,
        out_proj,
        xin,
        dyin,
        hidden.T,
        dgate.T,
        dup.T,
    )
    return (grad_gate.T[None], grad_up.T[None], grad_down[None], grad_out, grad_b, grad_c, grad_v)


def solution(mesh):
    in_specs = (
        P("sp", "tp"),
        P("sp", "tp"),
        P("sp", None),
        P("sp", None),
        P("sp", None, "tp"),
        P("sp", None, "tp"),
        P("sp", "tp", None),
        P(None, "tp"),
        P("sp", "tp"),
        P("sp", "tp"),
        P("sp", "tp"),
        P("sp", "tp"),
        P(None, "tp"),
    )
    out_specs = (
        P("sp", None, "tp"),
        P("sp", None, "tp"),
        P("sp", "tp", None),
        P("sp", "tp"),
        P("sp", "tp"),
        P("sp", "tp"),
        P("sp", "tp"),
    )
    return jax.shard_map(local, mesh=mesh, in_specs=in_specs, out_specs=out_specs, check_vma=False)
```

profile of v0, /device:TPU:1, one launch (start us, length us, event | category | flops | bytes accessed | tf_op | source)
XLA Modules:
  0.0 198.3 jit_solution(15530501565047938151)
XLA Ops:
  0.6 0.0 copy-start
  0.6 1.5 copy.20.w_ref
  2.2 82.8 %dispatch.1 = (bf16[512,2048]{1,0:T(8,128)(2,1)}, bf16[512,2048]{1,0:T(8,128)(2,1)}, bf16[512,128]{1,0:T(8,128)(2,1)}) custom-call(s32[2,128]{1,0:T(2,128)} %bitcast.67, f32[128,2]{1,0:T(8,128)} %copy.20.w_ref, bf16[128,256]{1,0:T(8,128)(2,1)} %x_ref.1, bf16[128,256]{1,0:T(8,128)(2,1)} %g_ref.3), custom_call_target="tpu_custom_call" | custom-call | tf_op jit(solution)/shard_map/dispatch/pallas_call | solution.py:171
  85.0 0.0 copy-done
  85.0 0.0 copy-start.1
  85.0 0.0 copy-start.11
  85.0 2.7 %fusion.2 = f32[512,352]{0,1:T(8,128)S(1)} fusion(bf16[512,2048]{1,0:T(8,128)(2,1)} %get-tuple-element.18.x_hbm, bf16[1,2048,352]{1,2,0:T(8,128)(2,1)S(1)} %copy-done), kind=kOutput, calls=%fused_computation.3 | convolution fusion | flops 738197504 | bytes 4259840 | tf_op jit(solution)/shard_map/dot_general | solution.py:499
  87.7 0.0 copy-done.1
  87.7 0.0 copy-done.11
  87.7 0.0 copy-start.2
  87.7 0.0 copy-start.12
  87.8 0.9 fusion.5
  88.7 0.6 copy-done.2
  89.3 0.4 copy-done.12
  89.7 1.2 fusion.11
  90.9 1.5 fusion
  92.4 0.0 copy-start.3
  92.4 0.0 copy-start.4
  92.4 0.0 copy-start.6
  92.4 0.0 copy-start.7
  92.4 0.0 copy-start.8
  92.4 0.0 copy-start.9
  92.4 0.0 copy-start.10
  92.4 1.4 add_convert_fusion.part_ref
  93.9 98.5 %combine.1 = (f32[64,256]{1,0:T(8,128)S(1)}, bf16[128,256]{1,0:T(8,128)(2,1)S(1)}, bf16[128,256]{1,0:T(8,128)(2,1)S(1)}, bf16[128,256]{1,0:T(8,128)(2,1)S(1)}, b...) custom-call(bf16[512,2048]{1,0:T(8,128)(2,1)S(1)} %add_convert_fusion.part_ref, ...), custom_call_target="tpu_custom_call" | custom-call | tf_op jit(solution)/shard_map/combine/pallas_call | solution.py:433
  192.4 1.1 copy.28
  193.5 1.1 copy.29
  194.6 1.1 copy.30
  195.7 0.6 copy.31
  196.4 0.6 copy.32
  197.0 0.6 copy.33
  197.6 0.6 copy.34
  (9 shorter events, 0.0 us)
Async XLA Ops:
  0.6 84.4 %copy-start = (bf16[1,2048,352]{1,2,0:T(8,128)(2,1)S(1)}, bf16[1,2048,352]{1,2,0:T(8,128)(2,1)}, u32[]{:S(2)}) copy-start(bf16[1,2048,352]{1,2,0:T(8,128)(2,1)} %param.17) | copy-start | bytes 4325380
  85.0 2.7 %copy-start.1 = (bf16[512,2048]{1,0:T(8,128)(2,1)S(1)}, bf16[512,2048]{1,0:T(8,128)(2,1)}, u32[]{:S(2)}) copy-start(bf16[512,2048]{1,0:T(8,128)(2,1)} %get-tuple-element.18.x_hbm) | copy-start | bytes 6291460
  85.0 2.7 %copy-start.11 = (bf16[1,2048,352]{1,2,0:T(8,128)(2,1)S(1)}, bf16[1,2048,352]{1,2,0:T(8,128)(2,1)}, u32[]{:S(2)}) copy-start(bf16[1,2048,352]{1,2,0:T(8,128)(2,1)} %param.18) | copy-start | bytes 4325380
  87.7 1.6 copy-start.2
  87.7 2.0 %copy-start.12 = (bf16[1,352,2048]{2,1,0:T(8,128)(2,1)S(1)}, bf16[1,352,2048]{2,1,0:T(8,128)(2,1)}, u32[]{:S(2)}) copy-start(bf16[1,352,2048]{2,1,0:T(8,128)(2,1)} %param.19) | copy-start | bytes 4325380
  92.4 1.5 copy-start.3
  92.4 1.5 copy-start.4
  92.4 1.5 copy-start.5
  92.4 1.5 copy-start.6
  92.4 1.5 copy-start.7
  92.4 1.5 copy-start.8
  92.4 1.5 copy-start.9
  92.4 1.5 copy-start.10
where the time goes:
time: 198 us
  Pallas kernels  181 us (91%)
  local copies, waits for them, and re-layouts  8.44 us (4%)
  matrix products  7.65 us (4%)
    pallas_call x1, Pallas kernels, combine(): pl.pallas_call(functools.partial(combine_kernel, n, q), out_shape=(jax.Sh...  98.5 us
    pallas_call x1, Pallas kernels, dispatch(): pl.pallas_call(functools.partial(dispatch_kernel, n, q), out_shape=(rows,...  82.8 us
    unnamed x34, local copies, waits for them, and re-layouts  8.44 us

commit v1 on v0

v1 whole, which is shorter than its diff:
```python
import functools

import jax
import jax.numpy as jnp
from jax import lax
from jax.experimental import pallas as pl
from jax.experimental.pallas import tpu as pltpu
from jax.sharding import PartitionSpec as P

MESH = pl.DeviceIdType.MESH
NX = 4
HALF = jnp.bfloat16
F32 = jnp.float32
DX = (0, 1, 3, 2)
NT = (((1,), (1,)), ((), ()))
NN = (((1,), (0,)), ((), ()))


def z_order(nz):
    near = [0]
    for d in range(1, nz // 2):
        near += [d, nz - d]
    return tuple(near + [nz // 2])


def remote(src, dst, send_sem, recv_sem, device):
    return pltpu.make_async_remote_copy(
        src_ref=src,
        dst_ref=dst,
        send_sem=send_sem,
        recv_sem=recv_sem,
        device_id=device,
        device_id_type=MESH,
    )


def step_kernel(
    n, q, ids_ref, w_ref, taps_ref, x_hbm, g_hbm, b_hbm, co_hbm, c_hbm, v_hbm, wg_hbm, wu_hbm, wd_hbm, wo_hbm,
    gout_ref, gb_ref, gc_ref, gv_ref, ggate_hbm, gup_hbm, gdown_hbm,
    x_v, g_v, b_v, co_v, c_v, v_v, wgu, wd, wo, p01, p_t, send, buf, mixed,
    hid_t, dgu_t, dgu, po, ps, rsib, pair, ryb, fin, ret, full_h, hx_send, hx, gpart, gr, edge, got, padded, ggate_v, gup_v, gdown_v,
    in_sem, out_sem, s1, r1, sy, ry, ss, rs, smx, rmx, sp, rp, sa, ra, sb, rb, shx, rhx, shy, rhy, shs, rhs,
    sqy, rqy, sqs, rqs, sgz, rgz, se, re,
):
    s, t = lax.axis_index("sp"), lax.axis_index("tp")
    sib = t + 1 - 2 * lax.rem(t, 2)
    z, x = lax.div(s, NX), lax.rem(s, NX)
    nz = n // NX
    ny = q // 2
    zs = z_order(nz)
    tok, cols = x_v.shape
    cap = 4 * tok // n
    total = n * cap
    units = wg_hbm.shape[0]
    high = wd.shape[0]
    share = q * cols // n
    hrows = total // 2

    def sp_at(dz, dx):
        return lax.rem(z + dz + nz, nz) * NX + lax.rem(x + dx + NX, NX)

    def tp_at(d):
        return lax.rem(t + 2 * d + q, q)

    barrier = pltpu.get_barrier_semaphore()
    peers = [(sp_at(dz, dx), t) for dz in zs for dx in DX][1:]
    peers += [(s, tp_at(d)) for d in range(1, ny)] + [(s, sib)]
    for peer in peers:
        pl.semaphore_signal(barrier, inc=1, device_id=peer, device_id_type=MESH)

    loads = [
        pltpu.make_async_copy(source, target, in_sem.at[k])
        for k, (source, target) in enumerate(
            [
                (x_hbm, x_v),
                (g_hbm, g_v),
                (b_hbm, b_v),
                (co_hbm, co_v),
                (wg_hbm, wgu.at[0:units]),
                (wu_hbm, wgu.at[high : high + units]),
                (wd_hbm, wd.at[0:units]),
                (wo_hbm, wo),
                (c_hbm, c_v),
                (v_hbm, v_v),
            ]
        )
    ]
    for load in loads:
        load.start()

    ids0, ids1 = ids_ref[0:1, :], ids_ref[1:2, :]
    experts = lax.broadcasted_iota(jnp.int32, (n, tok), 0)
    named = jnp.logical_or(ids0 == experts, ids1 == experts)
    earlier = jnp.where(
        lax.broadcasted_iota(jnp.int32, (tok, tok), 0) < lax.broadcasted_iota(jnp.int32, (tok, tok), 1), 1.0, 0.0
    )
    before = jnp.dot(
        jnp.where(named, 1.0, 0.0).astype(HALF), earlier.astype(HALF), preferred_element_type=F32
    ).astype(jnp.int32)
    slots = lax.broadcasted_iota(jnp.int32, (cap, tok), 0)
    for e in range(n):
        here = before[e : e + 1, :] == slots
        c0 = jnp.where(jnp.logical_and(here, ids0 == e), 1.0, 0.0)
        c1 = jnp.where(jnp.logical_and(here, ids1 == e), 1.0, 0.0)
        rows = slice(e * cap, (e + 1) * cap)
        p01[rows, 0:tok] = c0.astype(HALF)
        p01[rows, tok : 2 * tok] = c1.astype(HALF)
    loads[0].wait()
    loads[1].wait()
    grad = g_v[...].astype(F32)
    picked = p01[:, 0:tok] + p01[:, tok : 2 * tok]
    send[:, 0] = (
        jnp.dot(picked, x_v[...], preferred_element_type=F32).astype(HALF).reshape(n, cap, cols)
    )
    weighted = []
    for k in range(2):
        wide = jnp.broadcast_to(w_ref[k : k + 1, :], (tok, tok)).T
        wide = jnp.concatenate([wide] * (cols // tok), axis=1)
        weighted.append((wide * grad).astype(HALF))
    send[:, 1] = (
        jnp.dot(p01[...], jnp.concatenate(weighted, axis=0), preferred_element_type=F32)
        .astype(HALF)
        .reshape(n, cap, cols)
    )

    order = [(g, k) for g in range(nz) for k in range(NX)]

    def first(i):
        g, k = order[i]
        e = sp_at(zs[g], DX[k])
        return remote(send.at[e], buf.at[t, g, k], s1.at[i], r1.at[i], (e, t))

    def across(g, way):
        b = buf.at[t, g]
        return remote(b, b, sy.at[g, way], ry.at[g, way], (s, tp_at(1 - 2 * way)))

    def relay(g):
        way = g % 2
        b = buf.at[tp_at(2 * way - 1), g]
        return remote(b, b, sy.at[g, 2], ry.at[g, 2], (s, tp_at(1 - 2 * way)))

    def beside(g, d):
        b = buf.at[tp_at(-d), g]
        return remote(b, b, ss.at[g, d], rs.at[g, d], (s, sib))

    def mixed_x(k):
        return remote(mixed.at[0], mixed.at[k], smx.at[k], rmx.at[k], (sp_at(0, DX[k]), t))

    buf[t, 0, 0] = send[s]
    pl.semaphore_wait(barrier, len(peers))
    for i in range(1, n):
        first(i).start()
    loads[2].wait()
    loads[3].wait()
    mixed[0] = (b_v[...].astype(F32) * co_v[...].astype(F32)).astype(HALF)
    for k in range(1, NX):
        mixed_x(k).start()
    wgu[units:high, :] = jnp.zeros((high - units, q * cols), HALF)
    wgu[high + units : 2 * high, :] = jnp.zeros((high - units, q * cols), HALF)
    wd[units:high, :] = jnp.zeros((high - units, q * cols), HALF)
    p_t[...] = picked.astype(F32).T.astype(HALF)

    def forward(half):
        groups = slice(half * nz // 2, (half + 1) * nz // 2)
        here = slice(half * hrows, (half + 1) * hrows)
        xin = jnp.concatenate([buf[k, groups, :, 0].reshape(hrows, cols) for k in range(q)], axis=1)
        gu = lax.dot_general(wgu[...], xin, NT, preferred_element_type=F32)
        dyin = jnp.concatenate([buf[k, groups, :, 1].reshape(hrows, cols) for k in range(q)], axis=1)
        dhid = lax.dot_general(wd[...], dyin, NT, preferred_element_type=F32)
        gate, upval = gu[0:high], gu[high : 2 * high]
        sig = jax.nn.sigmoid(gate)
        act = gate * sig
        hid_t[:, here] = (act * upval).astype(HALF)
        dgate = dhid * upval * (sig * (1.0 + gate * (1.0 - sig)))
        dup = dhid * act
        dgu_t[0:high, here] = dgate.astype(HALF)
        dgu_t[high : 2 * high, here] = dup.astype(HALF)
        dgu[here, 0:high] = dgate.T.astype(HALF)
        dgu[here, high : 2 * high] = dup.T.astype(HALF)

    def take(g):
        across(g, 0).wait_recv()
        across(g, 1).wait_recv()
        relay(g).start()
        beside(g, 1).start()
        beside(g, ny - 1).start()

    def take_far(g):
        relay(g).wait_recv()
        beside(g, 2).start()

    def drain(g):
        for d in range(ny):
            beside(g, d).wait_recv()

    for g in range(nz):
        for i in range(g * NX, (g + 1) * NX):
            if i:
                first(i).wait_recv()
        across(g, 0).start()
        across(g, 1).start()
        beside(g, 0).start()
        if g >= 1:
            take(g - 1)
        if g >= 2:
            take_far(g - 2)
    for load in loads[4:]:
        load.wait()
    take(nz - 1)
    for g in range(nz // 2):
        drain(g)
    take_far(nz - 2)
    forward(0)
    take_far(nz - 1)
    for g in range(nz // 2, nz):
        drain(g)
    forward(1)

    def part(tt):
        here = pl.ds(pl.multiple_of(tt * cols, cols), cols)
        return jnp.dot(dgu[...], wgu[:, here], preferred_element_type=F32)

    def to_sib(d):
        return remote(ps.at[d], rsib.at[d], sp.at[d], rp.at[d], (s, sib))

    def reduce_y(g, d):
        return remote(pair.at[d, g], ryb.at[d, g], sa.at[g, d], ra.at[g, d], (s, tp_at(d)))

    def back(i):
        g, k = order[i]
        return remote(fin.at[g, k], ret.at[s], sb.at[i], rb.at[i], (sp_at(-zs[g], -DX[k]), t))

    ways = [2, *[d for d in range(1, ny) if d != 2], 0]
    blocks = (nz, NX, cap, cols)
    for d in ways:
        ps[d] = part(lax.rem(sib + 2 * d, q)).astype(HALF).reshape(blocks)
        to_sib(d).start()
    for d in ways:
        po[d] = part(tp_at(d)).astype(HALF).reshape(blocks)
    for d in ways:
        to_sib(d).wait_recv()
    for g in range(nz - 1, -1, -1):
        for d in ways:
            pair[d, g] = (po[d, g].astype(F32) + rsib[d, g].astype(F32)).astype(HALF)
            if d:
                reduce_y(g, d).start()

    def weight_grad(left, low, which, target):
        def step(k, _):
            here = pl.ds(pl.multiple_of(k * cols, cols), cols)
            target[:, here] = jnp.dot(
                left[low : low + units, :],
                buf[k, :, :, which].reshape(total, cols),
                preferred_element_type=F32,
            ).astype(HALF)
            return 0

        lax.fori_loop(0, q, step, 0)

    stores = [
        pltpu.make_async_copy(source, target, out_sem.at[k])
        for k, (source, target) in enumerate(
            [(gdown_v, gdown_hbm), (ggate_v, ggate_hbm), (gup_v, gup_hbm)]
        )
    ]
    weight_grad(hid_t, 0, 1, gdown_v)
    stores[0].start()
    weight_grad(dgu_t, 0, 0, ggate_v)
    stores[1].start()
    for g in range(nz - 1, -1, -1):
        value = pair[0, g].astype(F32)
        for d in range(1, ny):
            reduce_y(g, d).wait_recv()
            value = value + ryb[d, g].astype(F32)
        fin[g] = value.astype(HALF)
        for k in range(NX - 1, -1, -1):
            i = g * NX + k
            if i:
                back(i).start()
            else:
                ret[s] = fin[g, k]
    for i in range(n - 1, 0, -1):
        back(i).wait_recv()

    def h_across(d):
        b = full_h.at[t]
        return remote(b, b, shy.at[d], rhy.at[d], (s, tp_at(d)))

    def h_beside(d):
        b = full_h.at[tp_at(-d)]
        return remote(b, b, shs.at[d], rhs.at[d], (s, sib))

    def exchange(k):
        return remote(
            hx_send.at[lax.rem(x + DX[k], NX)], hx.at[t, k], shx.at[k], rhx.at[k], (sp_at(0, DX[k]), t)
        )

    def q_across(d):
        b = hx.at[t]
        return remote(b, b, sqy.at[d], rqy.at[d], (s, tp_at(d)))

    def q_beside(d):
        b = hx.at[tp_at(-d)]
        return remote(b, b, sqs.at[d], rqs.at[d], (s, sib))

    def term(k):
        zz = lax.rem(z + zs[k], nz)
        return remote(gpart.at[zz], gr.at[k], sgz.at[k], rgz.at[k], (zz * NX + x, t))

    def halo(k):
        there = lax.rem(s + 1, n) if k == 0 else lax.rem(s - 1 + n, n)
        return remote(edge.at[k], got.at[k], se.at[k], re.at[k], (there, t))

    moe = jnp.dot(p_t[...], ret[...].reshape(total, cols), preferred_element_type=F32)
    dh = g_v[...].astype(F32) + moe
    hx_send[...] = dh.T.astype(HALF).reshape(NX, share, tok)
    for k in range(1, NX):
        exchange(k).start()
    full_h[t] = dh.astype(HALF)
    for d in (2, *[d for d in range(1, ny) if d != 2]):
        h_across(d).start()
    h_beside(0).start()
    hx[t, 0] = hx_send[x]
    for k in range(1, NX):
        exchange(k).wait_recv()
    for d in (2, *[d for d in range(1, ny) if d != 2]):
        q_across(d).start()
    q_beside(0).start()
    for d in range(1, ny):
        h_across(d).wait_recv()
        h_beside(d).start()
    for d in range(ny):
        h_beside(d).wait_recv()
    dh_all = jnp.concatenate([full_h[k] for k in range(q)], axis=1)
    grad_z = jnp.dot(dh_all, wo[...], preferred_element_type=F32)
    dconv = (grad_z * b_v[...].astype(F32)).astype(HALF).astype(F32)
    edge[0] = jnp.broadcast_to(dconv[tok - 1 : tok, :], (8, cols))
    edge[1] = jnp.broadcast_to(dconv[0:1, :], (8, cols))
    halo(0).start()
    halo(1).start()
    gb_ref[...] = (grad_z * co_v[...].astype(F32)).astype(HALF)
    padded[8 : 8 + tok, :] = dconv
    for d in range(1, ny):
        q_across(d).wait_recv()
        q_beside(d).start()
    for k in range(1, NX):
        mixed_x(k).wait_recv()
    for d in range(ny):
        q_beside(d).wait_recv()
    left = jnp.concatenate([hx[:, k].reshape(q * share, tok) for k in range(NX)], axis=1)
    out = jnp.dot(left, mixed[...].reshape(NX * tok, cols), preferred_element_type=F32)
    gpart[...] = out.astype(HALF).reshape(nz, share, cols)
    for k in range(nz - 1, 0, -1):
        term(k).start()
    weight_grad(dgu_t, high, 0, gup_v)
    stores[2].start()
    halo(0).wait_recv()
    halo(1).wait_recv()
    padded[0:8, :] = jnp.where(s > 0, got[0], 0.0)
    padded[8 + tok : 16 + tok, :] = jnp.where(s < n - 1, got[1], 0.0)
    grad_u = (
        taps_ref[0:1, :] * padded[9 : 9 + tok, :]
        + taps_ref[1:2, :] * padded[8 : 8 + tok, :]
        + taps_ref[2:3, :] * padded[7 : 7 + tok, :]
    )
    gc_ref[...] = (grad_u * v_v[...].astype(F32)).astype(HALF)
    gv_ref[...] = (grad_u * c_v[...].astype(F32)).astype(HALF)
    sums = gpart[z].astype(F32)
    for k in range(1, nz):
        term(k).wait_recv()
        sums = sums + gr[k].astype(F32)
    gout_ref[...] = sums

    for store in stores:
        store.wait()
    for i in range(1, n):
        first(i).wait_send()
        back(i).wait_send()
    for g in range(nz):
        across(g, 0).wait_send()
        across(g, 1).wait_send()
        relay(g).wait_send()
        for d in range(ny):
            beside(g, d).wait_send()
            if d:
                reduce_y(g, d).wait_send()
    for k in range(1, NX):
        mixed_x(k).wait_send()
        exchange(k).wait_send()
    for d in range(ny):
        to_sib(d).wait_send()
        h_beside(d).wait_send()
        q_beside(d).wait_send()
        if d:
            h_across(d).wait_send()
            q_across(d).wait_send()
    for k in range(1, nz):
        term(k).wait_send()
    halo(0).wait_send()
    halo(1).wait_send()


def store_kernel(*refs):
    count = (len(refs) - 2) // 3
    reads = [pltpu.make_async_copy(refs[k], refs[2 * count + k], refs[-2].at[k]) for k in range(count)]
    writes = [pltpu.make_async_copy(refs[2 * count + k], refs[count + k], refs[-1].at[k]) for k in range(count)]
    for read in reads:
        read.start()
    for read, write in zip(reads, writes):
        read.wait()
        write.start()
    for write in writes:
        write.wait()


def local(
    out_grad,
    moe_input,
    route_weight,
    route_ids,
    gate_proj,
    up_proj,
    down_proj,
    out_proj,
    conv_out,
    gate_b,
    gate_c,
    value_v,
    conv_taps,
):
    n = lax.axis_size("sp")
    q = lax.axis_size("tp")
    tok, cols = moe_input.shape
    width = q * cols
    total = 4 * tok
    cap = total // n
    nz, ny = n // NX, q // 2
    units = down_proj.shape[1]
    high = -(-units // 128) * 128
    share = width // n
    vmem = pl.BlockSpec(memory_space=pltpu.VMEM)
    hbm = pl.BlockSpec(memory_space=pl.ANY)
    dma = pltpu.SemaphoreType.DMA
    blocks = (ny, nz, NX, cap, cols)

    def half(*shape):
        return pltpu.VMEM(shape, HALF)

    sems = [(n,), (nz, 3), (nz, ny), (NX,), (ny,), (nz, ny), (n,), (NX,), (ny,), (ny,), (ny,), (ny,), (nz,), (2,)]
    like = jax.ShapeDtypeStruct((tok, cols), HALF)
    tall = jax.ShapeDtypeStruct((units, width), HALF)
    shapes = (jax.ShapeDtypeStruct((share, cols), F32), like, like, like, tall, tall, tall)
    results = pl.pallas_call(
        functools.partial(step_kernel, n, q),
        out_shape=shapes,
        in_specs=[vmem] * 3 + [hbm] * 10,
        out_specs=(vmem,) * 4 + (hbm,) * 3,
        scratch_shapes=[half(tok, cols)] * 6
        + [
            half(2 * high, width),
            half(high, width),
            half(width, cols),
            half(total, 2 * tok),
            half(tok, total),
            half(n, 2, cap, cols),
            half(q, nz, NX, 2, cap, cols),
            half(NX, tok, cols),
            half(high, total),
            half(2 * high, total),
            half(total, 2 * high),
            half(*blocks),
            half(*blocks),
            half(*blocks),
            half(*blocks),
            half(*blocks),
            half(nz, NX, cap, cols),
            half(n, cap, cols),
            half(q, tok, cols),
            half(NX, share, tok),
            half(q, NX, share, tok),
            half(nz, share, cols),
            half(nz, share, cols),
            pltpu.VMEM((2, 8, cols), F32),
            pltpu.VMEM((2, 8, cols), F32),
            pltpu.VMEM((tok + 16, cols), F32),
            half(units, width),
            half(units, width),
            half(units, width),
            dma((10,)),
            dma((3,)),
        ]
        + [dma(shape) for shape in sems for _ in range(2)],
        compiler_params=pltpu.CompilerParams(
            collective_id=0, has_side_effects=True, vmem_limit_bytes=56 * 2**20
        ),
        name="step",
    )(
        route_ids.T,
        route_weight.T,
        conv_taps,
        moe_input,
        out_grad,
        gate_b,
        conv_out,
        gate_c,
        value_v,
        gate_proj[0].T,
        up_proj[0].T,
        down_proj[0],
        out_proj,
    )
    grad_out, grad_b, grad_c, grad_v, grad_gate, grad_up, grad_down = pl.pallas_call(
        store_kernel,
        out_shape=shapes,
        in_specs=[hbm] * 7,
        out_specs=(hbm,) * 7,
        scratch_shapes=[pltpu.VMEM(shape.shape, shape.dtype) for shape in shapes] + [dma((7,)), dma((7,))],
        name="store",
    )(*results)
    return (grad_gate.T[None], grad_up.T[None], grad_down[None], grad_out, grad_b, grad_c, grad_v)


def solution(mesh):
    in_specs = (
        P("sp", "tp"),
        P("sp", "tp"),
        P("sp", None),
        P("sp", None),
        P("sp", None, "tp"),
        P("sp", None, "tp"),
        P("sp", "tp", None),
        P(None, "tp"),
        P("sp", "tp"),
        P("sp", "tp"),
        P("sp", "tp"),
        P("sp", "tp"),
        P(None, "tp"),
    )
    out_specs = (
        P("sp", None, "tp"),
        P("sp", None, "tp"),
        P("sp", "tp", None),
        P("sp", "tp"),
        P("sp", "tp"),
        P("sp", "tp"),
        P("sp", "tp"),
    )
    return jax.shard_map(local, mesh=mesh, in_specs=in_specs, out_specs=out_specs, check_vma=False)
```

time: 198 us -> 93.5 us (0.47)
  Pallas kernels: 181 us -> 92.7 us
  local copies, waits for them, and re-layouts: 8.44 us -> 0 us
  matrix products: 7.65 us -> 0 us
    pallas_call x2, Pallas kernels: 181 us -> 92.7 us  [the longest x1 89 us: local(): pl.pallas_call(functools.partial(step_kernel, n, q), out_shape=shapes, in...]
    unnamed x34 -> x0, local copies, waits for them, and re-layouts: 8.44 us -> none
    dot_general x5 -> x0, matrix products: 7.65 us -> none  [the longest x1 2.68 us: local(): gate = jnp.dot(xin, w_gate, preferred_element_type=jnp.float32)]
where the time goes in v1:
time: 93.5 us; the launch traced here: 93.3 us
  Pallas kernels  92.7 us (99%)
    pallas_call x1, Pallas kernels, local(): pl.pallas_call(functools.partial(step_kernel, n, q), out_shape=shapes, in...  89 us
    pallas_call x1, Pallas kernels, local(): pl.pallas_call(store_kernel, out_shape=shapes, in_specs=[hbm] * 7, out_sp...  3.74 us

profile of v1, /device:TPU:1, one launch (start us, length us, event | category | flops | bytes accessed | tf_op | source)
XLA Modules:
  0.0 93.3 jit_solution(278769381450224399)
XLA Ops:
  0.6 89.0 %step.1 = (f32[64,256]{1,0:T(8,128)}, bf16[128,256]{1,0:T(8,128)(2,1)}, bf16[128,256]{1,0:T(8,128)(2,1)}, bf16[128,256]{1,0:T(8,128)(2,1)}, bf16[352,2048]{1,0:T...) custom-call(s32[2,128]{1,0:T(2,128)} %bitcast.19, f32[2,128]{1,0:T(2,128)} %bitcast.20, ...), custom_call_target="tpu_custom_call" | custom-call | tf_op jit(solution)/shard_map/step/pallas_call | solution.py:453
  89.6 3.7 %store.1 = (f32[64,256]{1,0:T(8,128)}, bf16[128,256]{1,0:T(8,128)(2,1)}, bf16[128,256]{1,0:T(8,128)(2,1)}, bf16[128,256]{1,0:T(8,128)(2,1)}, bf16[352,2048]{1,0:...) custom-call(f32[64,256]{1,0:T(8,128)} %get-tuple-element.21.refs_0_, ...), custom_call_target="tpu_custom_call" | custom-call | tf_op jit(solution)/shard_map/store/pallas_call | solution.py:512

commit v2 on v1

--- a/solution.py
+++ b/solution.py
@@ -35,12 +35,12 @@
 
 
 def step_kernel(
-    n, q, ids_ref, w_ref, taps_ref, x_hbm, g_hbm, b_hbm, co_hbm, c_hbm, v_hbm, wg_hbm, wu_hbm, wd_hbm, wo_hbm,
+    n, q, ids_hbm, w_hbm, taps_hbm, x_hbm, g_hbm, b_hbm, co_hbm, c_hbm, v_hbm, wg_hbm, wu_hbm, wd_hbm, wo_hbm,
     gout_ref, gb_ref, gc_ref, gv_ref, ggate_hbm, gup_hbm, gdown_hbm,
-    x_v, g_v, b_v, co_v, c_v, v_v, wgu, wd, wo, p01, p_t, send, buf, mixed,
+    ids_ref, w_ref, taps_ref, x_v, g_v, b_v, co_v, c_v, v_v, wgu, wd, wo, p01, p_t, send, buf, mixed,
     hid_t, dgu_t, dgu, po, ps, rsib, pair, ryb, fin, ret, full_h, hx_send, hx, gpart, gr, edge, got, padded, ggate_v, gup_v, gdown_v,
     in_sem, out_sem, s1, r1, sy, ry, ss, rs, smx, rmx, sp, rp, sa, ra, sb, rb, shx, rhx, shy, rhy, shs, rhs,
-    sqy, rqy, sqs, rqs, sgz, rgz, se, re,
+    sqs, rqs, sgz, rgz, se, re,
 ):
     s, t = lax.axis_index("sp"), lax.axis_index("tp")
     sib = t + 1 - 2 * lax.rem(t, 2)
@@ -62,9 +62,15 @@
     def tp_at(d):
         return lax.rem(t + 2 * d + q, q)
 
+    pending = []
+
+    def go(copy):
+        copy.start()
+        pending.append(copy)
+
     barrier = pltpu.get_barrier_semaphore()
-    peers = [(sp_at(dz, dx), t) for dz in zs for dx in DX][1:]
-    peers += [(s, tp_at(d)) for d in range(1, ny)] + [(s, sib)]
+    peers = [(sp_at(dz, dx), t) for dz in zs for dx in DX][:0:-1]
+    peers += [(sp_at(0, dx), tp_at(d)) for d in range(1, ny) for dx in DX] + [(s, sib)]
     for peer in peers:
         pl.semaphore_signal(barrier, inc=1, device_id=peer, device_id_type=MESH)
 
@@ -72,6 +78,8 @@
         pltpu.make_async_copy(source, target, in_sem.at[k])
         for k, (source, target) in enumerate(
             [
+                (ids_hbm, ids_ref),
+                (w_hbm, w_ref),
                 (x_hbm, x_v),
                 (g_hbm, g_v),
                 (b_hbm, b_v),
@@ -82,12 +90,15 @@
                 (wo_hbm, wo),
                 (c_hbm, c_v),
                 (v_hbm, v_v),
+                (taps_hbm, taps_ref),
             ]
         )
     ]
     for load in loads:
         load.start()
 
+    loads[0].wait()
+    loads[1].wait()
     ids0, ids1 = ids_ref[0:1, :], ids_ref[1:2, :]
     experts = lax.broadcasted_iota(jnp.int32, (n, tok), 0)
     named = jnp.logical_or(ids0 == experts, ids1 == experts)
@@ -105,8 +116,8 @@
         rows = slice(e * cap, (e + 1) * cap)
         p01[rows, 0:tok] = c0.astype(HALF)
         p01[rows, tok : 2 * tok] = c1.astype(HALF)
-    loads[0].wait()
-    loads[1].wait()
+    loads[2].wait()
+    loads[3].wait()
     grad = g_v[...].astype(F32)
     picked = p01[:, 0:tok] + p01[:, tok : 2 * tok]
     send[:, 0] = (
@@ -149,12 +160,12 @@
     buf[t, 0, 0] = send[s]
     pl.semaphore_wait(barrier, len(peers))
     for i in range(1, n):
-        first(i).start()
-    loads[2].wait()
-    loads[3].wait()
+        go(first(i))
+    loads[4].wait()
+    loads[5].wait()
     mixed[0] = (b_v[...].astype(F32) * co_v[...].astype(F32)).astype(HALF)
     for k in range(1, NX):
-        mixed_x(k).start()
+        go(mixed_x(k))
     wgu[units:high, :] = jnp.zeros((high - units, q * cols), HALF)
     wgu[high + units : 2 * high, :] = jnp.zeros((high - units, q * cols), HALF)
     wd[units:high, :] = jnp.zeros((high - units, q * cols), HALF)
@@ -178,50 +189,43 @@
         dgu[here, 0:high] = dgate.T.astype(HALF)
         dgu[here, high : 2 * high] = dup.T.astype(HALF)
 
+    def gathered(g):
+        for i in range(g * NX, (g + 1) * NX):
+            if i:
+                first(i).wait_recv()
+        go(across(g, 0))
+        go(across(g, 1))
+        go(beside(g, 0))
+
     def take(g):
-        across(g, 0).wait_recv()
-        across(g, 1).wait_recv()
-        relay(g).start()
-        beside(g, 1).start()
-        beside(g, ny - 1).start()
+        way = g % 2
+        across(g, way).wait_recv()
+        go(relay(g))
+        go(beside(g, 1 if way == 0 else ny - 1))
+        across(g, 1 - way).wait_recv()
+        go(beside(g, ny - 1 if way == 0 else 1))
 
     def take_far(g):
         relay(g).wait_recv()
-        beside(g, 2).start()
+        go(beside(g, 2))
 
     def drain(g):
         for d in range(ny):
             beside(g, d).wait_recv()
 
-    for g in range(nz):
-        for i in range(g * NX, (g + 1) * NX):
-            if i:
-                first(i).wait_recv()
-        across(g, 0).start()
-        across(g, 1).start()
-        beside(g, 0).start()
-        if g >= 1:
-            take(g - 1)
-        if g >= 2:
-            take_far(g - 2)
-    for load in loads[4:]:
-        load.wait()
-    take(nz - 1)
-    for g in range(nz // 2):
-        drain(g)
-    take_far(nz - 2)
-    forward(0)
-    take_far(nz - 1)
-    for g in range(nz // 2, nz):
-        drain(g)
-    forward(1)
-
-    def part(tt):
+    def part(tt, half):
         here = pl.ds(pl.multiple_of(tt * cols, cols), cols)
-        return jnp.dot(dgu[...], wgu[:, here], preferred_element_type=F32)
-
-    def to_sib(d):
-        return remote(ps.at[d], rsib.at[d], sp.at[d], rp.at[d], (s, sib))
+        value = jnp.dot(
+            dgu[half * hrows : (half + 1) * hrows, :], wgu[:, here], preferred_element_type=F32
+        )
+        return value.astype(HALF).reshape(nz // 2, NX, cap, cols)
+
+    def groups_of(half):
+        return pl.ds(half * nz // 2, nz // 2)
+
+    def to_sib(half, d):
+        here = groups_of(half)
+        return remote(ps.at[d, here], rsib.at[d, here], sp.at[half, d], rp.at[half, d], (s, sib))
 
     def reduce_y(g, d):
         return remote(pair.at[d, g], ryb.at[d, g], sa.at[g, d], ra.at[g, d], (s, tp_at(d)))
@@ -231,19 +235,48 @@
         return remote(fin.at[g, k], ret.at[s], sb.at[i], rb.at[i], (sp_at(-zs[g], -DX[k]), t))
 
     ways = [2, *[d for d in range(1, ny) if d != 2], 0]
-    blocks = (nz, NX, cap, cols)
-    for d in ways:
-        ps[d] = part(lax.rem(sib + 2 * d, q)).astype(HALF).reshape(blocks)
-        to_sib(d).start()
-    for d in ways:
-        po[d] = part(tp_at(d)).astype(HALF).reshape(blocks)
-    for d in ways:
-        to_sib(d).wait_recv()
-    for g in range(nz - 1, -1, -1):
+
+    def partial_sums(half):
+        here = slice(half * nz // 2, (half + 1) * nz // 2)
         for d in ways:
-            pair[d, g] = (po[d, g].astype(F32) + rsib[d, g].astype(F32)).astype(HALF)
-            if d:
-                reduce_y(g, d).start()
+            ps[d, here] = part(lax.rem(sib + 2 * d, q), half)
+            go(to_sib(half, d))
+        for d in ways:
+            po[d, here] = part(tp_at(d), half)
+
+    def send_pairs(half):
+        for d in ways:
+            to_sib(half, d).wait_recv()
+        for g in range((half + 1) * nz // 2 - 1, half * nz // 2 - 1, -1):
+            for d in ways:
+                pair[d, g] = (po[d, g].astype(F32) + rsib[d, g].astype(F32)).astype(HALF)
+                if d:
+                    go(reduce_y(g, d))
+
+    lead = nz // 2
+    for g in range(nz):
+        gathered(g)
+        if g >= lead - 1:
+            take(g - lead + 1)
+    for g in range(nz - lead + 1, nz):
+        take(g)
+        take_far(g - nz + lead - 1)
+    take_far(lead - 1)
+    for load in loads[6:]:
+        load.wait()
+    for g in range(lead):
+        drain(g)
+    forward(0)
+    for g in range(lead, nz - 1):
+        take_far(g)
+    partial_sums(0)
+    take_far(nz - 1)
+    send_pairs(0)
+    for g in range(lead, nz):
+        drain(g)
+    forward(1)
+    partial_sums(1)
+    send_pairs(1)
 
     def weight_grad(left, low, which, target):
         def step(k, _):
@@ -267,7 +300,9 @@
     stores[0].start()
     weight_grad(dgu_t, 0, 0, ggate_v)
     stores[1].start()
-    for g in range(nz - 1, -1, -1):
+    weight_grad(dgu_t, high, 0, gup_v)
+    stores[2].start()
+    for g in [*range(lead - 1, -1, -1), *range(nz - 1, lead - 1, -1)]:
         value = pair[0, g].astype(F32)
         for d in range(1, ny):
             reduce_y(g, d).wait_recv()
@@ -276,7 +311,7 @@
         for k in range(NX - 1, -1, -1):
             i = g * NX + k
             if i:
-                back(i).start()
+                go(back(i))
             else:
                 ret[s] = fin[g, k]
     for i in range(n - 1, 0, -1):
@@ -290,14 +325,14 @@
         b = full_h.at[tp_at(-d)]
         return remote(b, b, shs.at[d], rhs.at[d], (s, sib))
 
-    def exchange(k):
+    def exchange(d, k):
         return remote(
-            hx_send.at[lax.rem(x + DX[k], NX)], hx.at[t, k], shx.at[k], rhx.at[k], (sp_at(0, DX[k]), t)
+            hx_send.at[lax.rem(x + DX[k], NX)],
+            hx.at[t, k],
+            shx.at[d, k],
+            rhx.at[d, k],
+            (sp_at(0, DX[k]), tp_at(d)),
         )
-
-    def q_across(d):
-        b = hx.at[t]
-        return remote(b, b, sqy.at[d], rqy.at[d], (s, tp_at(d)))
 
     def q_beside(d):
         b = hx.at[tp_at(-d)]
@@ -314,46 +349,43 @@
     moe = jnp.dot(p_t[...], ret[...].reshape(total, cols), preferred_element_type=F32)
     dh = g_v[...].astype(F32) + moe
     hx_send[...] = dh.T.astype(HALF).reshape(NX, share, tok)
+    for d in ways:
+        for k in range(NX - 1, -1, -1):
+            if d or k:
+                go(exchange(d, k))
+    full_h[t] = dh.astype(HALF)
+    for d in ways[:-1]:
+        go(h_across(d))
+    go(h_beside(0))
+    hx[t, 0] = hx_send[x]
+    for d in ways[::-1]:
+        for k in range(NX):
+            if d or k:
+                exchange(d, k).wait_recv()
+        go(q_beside(d))
+    for d in ways[-2::-1]:
+        h_across(d).wait_recv()
+        go(h_beside(d))
     for k in range(1, NX):
-        exchange(k).start()
-    full_h[t] = dh.astype(HALF)
-    for d in (2, *[d for d in range(1, ny) if d != 2]):
-        h_across(d).start()
-    h_beside(0).start()
-    hx[t, 0] = hx_send[x]
-    for k in range(1, NX):
-        exchange(k).wait_recv()
-    for d in (2, *[d for d in range(1, ny) if d != 2]):
-        q_across(d).start()
-    q_beside(0).start()
-    for d in range(1, ny):
-        h_across(d).wait_recv()
-        h_beside(d).start()
-    for d in range(ny):
+        mixed_x(k).wait_recv()
+    for d in ways[::-1]:
+        q_beside(d).wait_recv()
+    left = jnp.concatenate([hx[:, k].reshape(q * share, tok) for k in range(NX)], axis=1)
+    out = jnp.dot(left, mixed[...].reshape(NX * tok, cols), preferred_element_type=F32)
+    gpart[...] = out.astype(HALF).reshape(nz, share, cols)
+    for k in range(nz - 1, 0, -1):
+        go(term(k))
+    for d in ways[::-1]:
         h_beside(d).wait_recv()
     dh_all = jnp.concatenate([full_h[k] for k in range(q)], axis=1)
     grad_z = jnp.dot(dh_all, wo[...], preferred_element_type=F32)
     dconv = (grad_z * b_v[...].astype(F32)).astype(HALF).astype(F32)
     edge[0] = jnp.broadcast_to(dconv[tok - 1 : tok, :], (8, cols))
     edge[1] = jnp.broadcast_to(dconv[0:1, :], (8, cols))
-    halo(0).start()
-    halo(1).start()
+    go(halo(0))
+    go(halo(1))
     gb_ref[...] = (grad_z * co_v[...].astype(F32)).astype(HALF)
     padded[8 : 8 + tok, :] = dconv
-    for d in range(1, ny):
-        q_across(d).wait_recv()
-        q_beside(d).start()
-    for k in range(1, NX):
-        mixed_x(k).wait_recv()
-    for d in range(ny):
-        q_beside(d).wait_recv()
-    left = jnp.concatenate([hx[:, k].reshape(q * share, tok) for k in range(NX)], axis=1)
-    out = jnp.dot(left, mixed[...].reshape(NX * tok, cols), preferred_element_type=F32)
-    gpart[...] = out.astype(HALF).reshape(nz, share, cols)
-    for k in range(nz - 1, 0, -1):
-        term(k).start()
-    weight_grad(dgu_t, high, 0, gup_v)
-    stores[2].start()
     halo(0).wait_recv()
     halo(1).wait_recv()
     padded[0:8, :] = jnp.where(s > 0, got[0], 0.0)
@@ -373,37 +405,17 @@
 
     for store in stores:
         store.wait()
-    for i in range(1, n):
-        first(i).wait_send()
-        back(i).wait_send()
-    for g in range(nz):
-        across(g, 0).wait_send()
-        across(g, 1).wait_send()
-        relay(g).wait_send()
-        for d in range(ny):
-            beside(g, d).wait_send()
-            if d:
-                reduce_y(g, d).wait_send()
-    for k in range(1, NX):
-        mixed_x(k).wait_send()
-        exchange(k).wait_send()
-    for d in range(ny):
-        to_sib(d).wait_send()
-        h_beside(d).wait_send()
-        q_beside(d).wait_send()
-        if d:
-            h_across(d).wait_send()
-            q_across(d).wait_send()
-    for k in range(1, nz):
-        term(k).wait_send()
-    halo(0).wait_send()
-    halo(1).wait_send()
+    for copy in pending:
+        copy.wait_send()
 
 
 def store_kernel(*refs):
     count = (len(refs) - 2) // 3
-    reads = [pltpu.make_async_copy(refs[k], refs[2 * count + k], refs[-2].at[k]) for k in range(count)]
-    writes = [pltpu.make_async_copy(refs[2 * count + k], refs[count + k], refs[-1].at[k]) for k in range(count)]
+    reads, writes = [], []
+    for k in [*range(4, count), *range(4)]:
+        held = refs[2 * count + k]
+        reads.append(pltpu.make_async_copy(refs[k], held, refs[-2].at[k]))
+        writes.append(pltpu.make_async_copy(held, refs[count + k], refs[-1].at[k]))
     for read in reads:
         read.start()
     for read, write in zip(reads, writes):
@@ -446,16 +458,17 @@
     def half(*shape):
         return pltpu.VMEM(shape, HALF)
 
-    sems = [(n,), (nz, 3), (nz, ny), (NX,), (ny,), (nz, ny), (n,), (NX,), (ny,), (ny,), (ny,), (ny,), (nz,), (2,)]
+    sems = [(n,), (nz, 3), (nz, ny), (NX,), (2, ny), (nz, ny), (n,), (ny, NX), (ny,), (ny,), (ny,), (nz,), (2,)]
     like = jax.ShapeDtypeStruct((tok, cols), HALF)
     tall = jax.ShapeDtypeStruct((units, width), HALF)
     shapes = (jax.ShapeDtypeStruct((share, cols), F32), like, like, like, tall, tall, tall)
     results = pl.pallas_call(
         functools.partial(step_kernel, n, q),
         out_shape=shapes,
-        in_specs=[vmem] * 3 + [hbm] * 10,
+        in_specs=[hbm] * 13,
         out_specs=(vmem,) * 4 + (hbm,) * 3,
-        scratch_shapes=[half(tok, cols)] * 6
+        scratch_shapes=[pltpu.VMEM((2, tok), jnp.int32), pltpu.VMEM((2, tok), F32), pltpu.VMEM((3, cols), F32)]
+        + [half(tok, cols)] * 6
         + [
             half(2 * high, width),
             half(high, width),
@@ -486,7 +499,7 @@
             half(units, width),
             half(units, width),
             half(units, width),
-            dma((10,)),
+            dma((13,)),
             dma((3,)),
         ]
         + [dma(shape) for shape in sems for _ in range(2)],

time: 93.5 us -> 84.8 us (0.907)
  Pallas kernels: 92.7 us -> 84 us
    pallas_call x1, Pallas kernels: 89 us -> 80.4 us  [local(): pl.pallas_call(functools.partial(step_kernel, n, q), out_shape=shapes, in...]
where the time goes in v2:
time: 84.8 us; the launch traced here: 84.7 us
  Pallas kernels  84 us (99%)
    pallas_call x1, Pallas kernels, local(): pl.pallas_call(functools.partial(step_kernel, n, q), out_shape=shapes, in...  80.4 us
    pallas_call x1, Pallas kernels, local(): pl.pallas_call(store_kernel, out_shape=shapes, in_specs=[hbm] * 7, out_sp...  3.6 us

profile of v2, /device:TPU:1, one launch (start us, length us, event | category | flops | bytes accessed | tf_op | source)
XLA Modules:
  0.0 84.7 jit_solution(5659371672801129919)
XLA Ops:
  0.6 80.4 %step.1 = (f32[64,256]{1,0:T(8,128)}, bf16[128,256]{1,0:T(8,128)(2,1)}, bf16[128,256]{1,0:T(8,128)(2,1)}, bf16[128,256]{1,0:T(8,128)(2,1)}, bf16[352,2048]{1,0:T...) custom-call(s32[2,128]{1,0:T(2,128)} %bitcast.19, f32[2,128]{1,0:T(2,128)} %bitcast.20, ...), custom_call_target="tpu_custom_call" | custom-call | tf_op jit(solution)/shard_map/step/pallas_call | solution.py:465
  81.1 3.6 %store.1 = (f32[64,256]{1,0:T(8,128)}, bf16[128,256]{1,0:T(8,128)(2,1)}, bf16[128,256]{1,0:T(8,128)(2,1)}, bf16[128,256]{1,0:T(8,128)(2,1)}, bf16[352,2048]{1,0:...) custom-call(f32[64,256]{1,0:T(8,128)} %get-tuple-element.21.refs_0_, ...), custom_call_target="tpu_custom_call" | custom-call | tf_op jit(solution)/shard_map/store/pallas_call | solution.py:525

commit v3 on v2

--- a/solution.py
+++ b/solution.py
@@ -298,10 +298,6 @@
     ]
     weight_grad(hid_t, 0, 1, gdown_v)
     stores[0].start()
-    weight_grad(dgu_t, 0, 0, ggate_v)
-    stores[1].start()
-    weight_grad(dgu_t, high, 0, gup_v)
-    stores[2].start()
     for g in [*range(lead - 1, -1, -1), *range(nz - 1, lead - 1, -1)]:
         value = pair[0, g].astype(F32)
         for d in range(1, ny):
@@ -358,6 +354,8 @@
         go(h_across(d))
     go(h_beside(0))
     hx[t, 0] = hx_send[x]
+    weight_grad(dgu_t, 0, 0, ggate_v)
+    stores[1].start()
     for d in ways[::-1]:
         for k in range(NX):
             if d or k:
@@ -384,6 +382,8 @@
     edge[1] = jnp.broadcast_to(dconv[0:1, :], (8, cols))
     go(halo(0))
     go(halo(1))
+    weight_grad(dgu_t, high, 0, gup_v)
+    stores[2].start()
     gb_ref[...] = (grad_z * co_v[...].astype(F32)).astype(HALF)
     padded[8 : 8 + tok, :] = dconv
     halo(0).wait_recv()

time: 84.8 us -> 81.4 us (0.960)
  Pallas kernels: 84 us -> 80.6 us
    pallas_call x1, Pallas kernels: 80.4 us -> 77 us  [local(): pl.pallas_call(functools.partial(step_kernel, n, q), out_shape=shapes, in...]
where the time goes in v3:
time: 81.4 us; the launch traced here: 81.3 us
  Pallas kernels  80.6 us (99%)
    pallas_call x1, Pallas kernels, local(): pl.pallas_call(functools.partial(step_kernel, n, q), out_shape=shapes, in...  77 us
    pallas_call x1, Pallas kernels, local(): pl.pallas_call(store_kernel, out_shape=shapes, in_specs=[hbm] * 7, out_sp...  3.6 us

profile of v3, /device:TPU:1, one launch (start us, length us, event | category | flops | bytes accessed | tf_op | source)
XLA Modules:
  0.0 81.3 jit_solution(910452504111528189)
XLA Ops:
  0.6 77.0 %step.1 = (f32[64,256]{1,0:T(8,128)}, bf16[128,256]{1,0:T(8,128)(2,1)}, bf16[128,256]{1,0:T(8,128)(2,1)}, bf16[128,256]{1,0:T(8,128)(2,1)}, bf16[352,2048]{1,0:T...) custom-call(s32[2,128]{1,0:T(2,128)} %bitcast.19, f32[2,128]{1,0:T(2,128)} %bitcast.20, ...), custom_call_target="tpu_custom_call" | custom-call | tf_op jit(solution)/shard_map/step/pallas_call | solution.py:465
  77.7 3.6 %store.1 = (f32[64,256]{1,0:T(8,128)}, bf16[128,256]{1,0:T(8,128)(2,1)}, bf16[128,256]{1,0:T(8,128)(2,1)}, bf16[128,256]{1,0:T(8,128)(2,1)}, bf16[352,2048]{1,0:...) custom-call(f32[64,256]{1,0:T(8,128)} %get-tuple-element.21.refs_0_, ...), custom_call_target="tpu_custom_call" | custom-call | tf_op jit(solution)/shard_map/store/pallas_call | solution.py:525

commit v4 on v3

--- a/solution.py
+++ b/solution.py
@@ -296,8 +296,6 @@
             [(gdown_v, gdown_hbm), (ggate_v, ggate_hbm), (gup_v, gup_hbm)]
         )
     ]
-    weight_grad(hid_t, 0, 1, gdown_v)
-    stores[0].start()
     for g in [*range(lead - 1, -1, -1), *range(nz - 1, lead - 1, -1)]:
         value = pair[0, g].astype(F32)
         for d in range(1, ny):
@@ -310,6 +308,8 @@
                 go(back(i))
             else:
                 ret[s] = fin[g, k]
+    weight_grad(hid_t, 0, 1, gdown_v)
+    stores[0].start()
     for i in range(n - 1, 0, -1):
         back(i).wait_recv()
 
@@ -336,7 +336,7 @@
 
     def term(k):
         zz = lax.rem(z + zs[k], nz)
-        return remote(gpart.at[zz], gr.at[k], sgz.at[k], rgz.at[k], (zz * NX + x, t))
+        return remote(gpart.at[k], gr.at[k], sgz.at[k], rgz.at[k], (zz * NX + x, t))
 
     def halo(k):
         there = lax.rem(s + 1, n) if k == 0 else lax.rem(s - 1 + n, n)
@@ -368,11 +368,16 @@
         mixed_x(k).wait_recv()
     for d in ways[::-1]:
         q_beside(d).wait_recv()
-    left = jnp.concatenate([hx[:, k].reshape(q * share, tok) for k in range(NX)], axis=1)
-    out = jnp.dot(left, mixed[...].reshape(NX * tok, cols), preferred_element_type=F32)
-    gpart[...] = out.astype(HALF).reshape(nz, share, cols)
-    for k in range(nz - 1, 0, -1):
-        go(term(k))
+    for low in (nz // 2, 0):
+        held = [hx[lax.rem(z + zs[low + j], nz)] for j in range(nz // 2)]
+        left = jnp.concatenate(
+            [jnp.concatenate([block[k] for k in range(NX)], axis=1) for block in held], axis=0
+        )
+        out = jnp.dot(left, mixed[...].reshape(NX * tok, cols), preferred_element_type=F32)
+        gpart[low : low + nz // 2] = out.astype(HALF).reshape(nz // 2, share, cols)
+        for k in range(low + nz // 2 - 1, low - 1, -1):
+            if k:
+                go(term(k))
     for d in ways[::-1]:
         h_beside(d).wait_recv()
     dh_all = jnp.concatenate([full_h[k] for k in range(q)], axis=1)
@@ -397,7 +402,7 @@
     )
     gc_ref[...] = (grad_u * v_v[...].astype(F32)).astype(HALF)
     gv_ref[...] = (grad_u * c_v[...].astype(F32)).astype(HALF)
-    sums = gpart[z].astype(F32)
+    sums = gpart[0].astype(F32)
     for k in range(1, nz):
         term(k).wait_recv()
         sums = sums + gr[k].astype(F32)

time: 81.4 us -> 81.3 us (level)
  no operation moved by 1% of the time
where the time goes in v4:
time: 81.3 us; the launch traced here: 81.2 us
  Pallas kernels  80.6 us (99%)
    pallas_call x1, Pallas kernels, local(): pl.pallas_call(functools.partial(step_kernel, n, q), out_shape=shapes, in...  77 us
    pallas_call x1, Pallas kernels, local(): pl.pallas_call(store_kernel, out_shape=shapes, in_specs=[hbm] * 7, out_sp...  3.6 us

profile of v4, /device:TPU:1, one launch (start us, length us, event | category | flops | bytes accessed | tf_op | source)
XLA Modules:
  0.0 81.2 jit_solution(16452051774393319968)
XLA Ops:
  0.6 77.0 %step.1 = (f32[64,256]{1,0:T(8,128)}, bf16[128,256]{1,0:T(8,128)(2,1)}, bf16[128,256]{1,0:T(8,128)(2,1)}, bf16[128,256]{1,0:T(8,128)(2,1)}, bf16[352,2048]{1,0:T...) custom-call(s32[2,128]{1,0:T(2,128)} %bitcast.19, f32[2,128]{1,0:T(2,128)} %bitcast.20, ...), custom_call_target="tpu_custom_call" | custom-call | tf_op jit(solution)/shard_map/step/pallas_call | solution.py:470
  77.6 3.6 %store.1 = (f32[64,256]{1,0:T(8,128)}, bf16[128,256]{1,0:T(8,128)(2,1)}, bf16[128,256]{1,0:T(8,128)(2,1)}, bf16[128,256]{1,0:T(8,128)(2,1)}, bf16[352,2048]{1,0:...) custom-call(f32[64,256]{1,0:T(8,128)} %get-tuple-element.21.refs_0_, ...), custom_call_target="tpu_custom_call" | custom-call | tf_op jit(solution)/shard_map/store/pallas_call | solution.py:530
